TPU v7x, 512 devices: a whole 4x4x16 slice. The times are simulated.
512 devices in a mesh: sp: 64 (over z, y), tp: 8 (over x, core).
Axes of the slice: x: 4, y: 4, z: 16, core: 2. Of those that a mesh axis runs over, the one named last changes fastest.
Arguments:
- tokens: bfloat16 [24576, 2048], P(('sp', 'tp')), may hold values from -6 to 6
- norm_gain: float32 [2048], replicated, may hold values from 0.1 to 1.9
- conv_in_weight: bfloat16 [2048, 2048], P('sp', 'tp'), may hold values from -0.125 to 0.125
- conv_gate_weight: bfloat16 [2048, 2048], P('sp', 'tp'), may hold values from -0.125 to 0.125
- conv_taps: float32 [3, 2048], replicated, may hold values from -3 to 3
- query_weight: bfloat16 [2048, 1024], P('sp', 'tp'), may hold values from -0.125 to 0.125
- key_weight: bfloat16 [2048, 1024], P('sp', 'tp'), may hold values from -0.125 to 0.125
- value_weight: bfloat16 [2048, 2048], P('sp', 'tp'), may hold values from -0.125 to 0.125
- decay_down: bfloat16 [2048, 16], replicated, may hold values from -0.125 to 0.125
- decay_up: bfloat16 [16, 1024], replicated, may hold values from -1.5 to 1.5
- decay_bias: float32 [1024], replicated, may hold values from 0.2 to 10
- decay_extra: float32 [8, 24576], P('tp', 'sp'), may hold values from -2.2 to 0
- head_gain: float32 [2048], replicated, may hold values from 0.1 to 1.9
- conv_out_weight: bfloat16 [2048, 2048], P('tp', 'sp'), may hold values from -0.125 to 0.125
- value_out_weight: bfloat16 [2048, 2048], P('tp', 'sp'), may hold values from -0.125 to 0.125
Outputs:
- mixed: bfloat16 [24576, 2048], P(('sp', 'tp'))
All inputs are finite; a program needn't handle non-finite values.
Results may differ from a plain program's by a relative error of at most 0.02.
Values may be sent and summed in bfloat16 or wider, within the bound.
A program may use at most 64 MiB of HBM per device.

v0:
```python
import math
import jax
import jax.numpy as jnp
from jax import lax
from jax.sharding import Mesh
from jax.sharding import PartitionSpec as P

KEY_DIM = 128
VAL_DIM = 256
BLOCK = 64
SP = ("sp_0", "sp_1")
SP_TP = ("sp_0", "sp_1", "tp")
EPSILON = 1e-06


def nothing_yet(array, identity):
    return jax.tree.map(
        lambda part, zero: jnp.zeros_like(part) + jnp.asarray(zero, part.dtype), array, identity
    )


def prefix_by_axis(array, axes, combine, identity, reverse):
    before = start = nothing_yet(array, identity)
    subtotal = array
    for axis in reversed(axes):
        count, place = (lax.axis_size(axis), lax.axis_index(axis))
        pieces = jax.tree.map(
            lambda part, kind: lax.all_gather(part.astype(kind), axis),
            subtotal,
            (jnp.bfloat16, jnp.bfloat16),
        )
        inside, subtotal = (start, start)
        for k in reversed(range(count)) if reverse else range(count):
            passed = k > place if reverse else k < place
            subtotal = combine(
                subtotal, jax.tree.map(lambda part, own: part[k].astype(own.dtype), pieces, array)
            )
            inside = jax.tree.map(lambda new, old: jnp.where(passed, new, old), subtotal, inside)
        before = combine(inside, before)
    return before


def copy_for_each(array, axis):
    count = lax.axis_size(axis)
    return lax.all_to_all(
        jnp.broadcast_to(array[None], (count, *array.shape)), axis, 0, 0, tiled=True
    )


def joined_along(blocks, dim):
    blocks = jnp.moveaxis(blocks, 0, dim)
    dims = blocks.shape
    return blocks.reshape(*dims[:dim], dims[dim] * dims[dim + 1], *dims[dim + 2 :])


def gathered_copies(array, axis, dim):
    blocks = copy_for_each(array, axis)
    return joined_along(blocks, dim)


def rows_first(arrays, axis, dims):
    turned = [jnp.moveaxis(a, dim, 0) for a, dim in zip(arrays, dims)]
    widths = [t[0].size for t in turned]
    both = jnp.concatenate([t.reshape(-1, w) for t, w in zip(turned, widths)], axis=1)
    filled = lax.all_gather(both, axis, axis=0, tiled=True)
    blocks = jnp.split(filled, [sum(widths[:k]) for k in range(1, len(widths))], axis=1)
    return tuple(
        (
            jnp.moveaxis(b.reshape(-1, *t.shape[1:]), 0, dim)
            for b, t, dim in zip(blocks, turned, dims)
        )
    )


def padded_2(block, sides, width):
    for axis, dim in sides:
        count = lax.axis_size(axis)
        forward = [(i, i + 1) for i in range(count - 1)]
        backward = [(target, source) for source, target in forward]
        low = lax.ppermute(
            lax.slice_in_dim(block, block.shape[dim] - width, None, axis=dim), axis, forward
        )
        high = lax.ppermute(lax.slice_in_dim(block, 0, width, axis=dim), axis, backward)
        block = jnp.concatenate([low, block, high], axis=dim)
    return block


def cut_along(array, dim, count):
    before, after = (array.shape[:dim], array.shape[dim + 1 :])
    return jnp.moveaxis(array.reshape(*before, count, -1, *after), dim, 0)


def sum_at_owner(array, axis, dim):
    blocks = cut_along(array, dim, lax.axis_size(axis))
    arrived = lax.all_to_all(blocks, axis, split_axis=0, concat_axis=0, tiled=True)
    return arrived.astype(jnp.float32).sum(axis=0)


def rms_rows(inputs, scale_gain):
    floats = inputs.astype(jnp.float32)
    return (
        floats * lax.rsqrt(jnp.mean(floats * floats, axis=-1, keepdims=True) + EPSILON) * scale_gain
    )


def rounded(inputs):
    return lax.optimization_barrier(inputs.astype(jnp.bfloat16)).astype(jnp.float32)


def project(normed, weight):
    return jnp.dot(normed, weight, preferred_element_type=jnp.float32)


def chain_combine(earlier, later):
    return (earlier[0] * later[0], later[0][..., None] * earlier[1] + later[1])


def gla_heads(queries, key_rows, values, log_decay):
    length, head_count, key_dim = queries.shape
    val_dim = values.shape[-1]
    blocks = length // BLOCK
    query_float = queries.astype(jnp.float32).reshape(blocks, BLOCK, head_count, key_dim)
    key_float = key_rows.astype(jnp.float32).reshape(blocks, BLOCK, head_count, key_dim)
    value_float = values.astype(jnp.float32).reshape(blocks, BLOCK, head_count, val_dim)
    decay_blocks = log_decay.reshape(blocks, BLOCK, head_count, key_dim)
    cumul = jnp.cumsum(decay_blocks, axis=1)
    before = cumul - decay_blocks
    totals = cumul[:, -1]
    offsets = jnp.cumsum(totals, axis=0) - totals
    whole_decay = jnp.sum(totals, axis=0)
    element_indices = jnp.arange(BLOCK)
    lower_mask = element_indices[:, None] >= element_indices[None, :]
    fwd_query = query_float * jnp.exp(cumul)
    fwd_scores = jnp.einsum("nihd,njhd->nhij", fwd_query, key_float * jnp.exp(-cumul))
    fwd_scores = jnp.where(lower_mask, fwd_scores, 0.0)
    key_start = key_float * jnp.exp(before)
    back_scores = jnp.einsum("nihd,njhd->nhij", query_float * jnp.exp(-before), key_start)
    back_scores = jnp.where(lower_mask.T, back_scores, 0.0)
    within = jnp.einsum("nhij,njhe->nihe", fwd_scores + back_scores, value_float)
    fwd_inc = jnp.einsum(
        "njhd,njhe->nhde", key_float * jnp.exp(totals[:, None] - cumul), value_float
    )
    back_inc = jnp.einsum("njhd,njhe->nhde", key_start, value_float)
    tail_decay = jnp.exp(whole_decay[None] - offsets - totals)
    fwd_device = jnp.einsum("nhd,nhde->hde", tail_decay, fwd_inc)
    back_device = jnp.einsum("nhd,nhde->hde", jnp.exp(offsets), back_inc)
    identity = (jnp.ones_like(whole_decay), jnp.zeros_like(fwd_device))
    incoming_fwd = prefix_by_axis(
        (jnp.exp(whole_decay), fwd_device), SP, chain_combine, identity, False
    )[1]
    incoming_back = prefix_by_axis(
        (jnp.exp(whole_decay), back_device), SP, chain_combine, identity, True
    )[1]
    block_order = jnp.arange(blocks)
    earlier_mask = (block_order[:, None] > block_order[None, :])[:, :, None, None]
    gap_fwd = offsets[:, None] - offsets[None, :] - totals[None, :]
    weights_fwd = jnp.exp(jnp.where(earlier_mask, gap_fwd, -jnp.inf))
    starts_fwd = (
        jnp.einsum("bchd,chde->bhde", weights_fwd, fwd_inc)
        + jnp.exp(offsets)[..., None] * incoming_fwd[None]
    )
    later_mask = (block_order[:, None] < block_order[None, :])[:, :, None, None]
    gap_back = offsets[None, :] - offsets[:, None] - totals[:, None]
    weights_back = jnp.exp(jnp.where(later_mask, gap_back, -jnp.inf))
    next_back = (
        jnp.einsum("bchd,chde->bhde", weights_back, back_inc)
        + tail_decay[..., None] * incoming_back[None]
    )
    carried_terms = jnp.einsum("nihd,nhde->nihe", fwd_query, starts_fwd)
    carried_terms = carried_terms + jnp.einsum(
        "nihd,nhde->nihe", query_float * jnp.exp(totals[:, None] - before), next_back
    )
    return (within + carried_terms).reshape(length, head_count, val_dim)


def local(
    tokens,
    norm_gain,
    conv_in_weight,
    conv_gate_weight,
    conv_taps,
    query_weight,
    key_weight,
    value_weight,
    decay_down,
    decay_up,
    decay_bias,
    decay_extra,
    head_gain,
    conv_out_weight,
    value_out_weight,
):
    shard_index = lax.axis_index("tp")
    channels = conv_in_weight.shape[1]
    key_width = query_weight.shape[1]
    val_width = value_weight.shape[1]
    head_count = decay_extra.shape[0]
    gathered = gathered_copies(tokens, "tp", 0)
    normed = rms_rows(gathered, norm_gain).astype(jnp.bfloat16)
    length = normed.shape[0]
    gathered_weights = rows_first(
        (
            conv_in_weight,
            conv_gate_weight,
            query_weight,
            key_weight,
            value_weight,
            conv_out_weight,
            value_out_weight,
        ),
        SP,
        (0, 0, 0, 0, 0, 1, 1),
    )
    conv_pre = project(normed, gathered_weights[0])
    gate_pre = project(normed, gathered_weights[1])
    probe_before_norm = project(normed, gathered_weights[2])
    key_pre = project(normed, gathered_weights[3])
    value_pre = project(normed, gathered_weights[4])
    conv_out_full = gathered_weights[5]
    value_out_full = gathered_weights[6]
    conv_in = conv_pre.astype(jnp.bfloat16)
    padded = padded_2(conv_in, ((SP, 0),), 1).astype(jnp.float32)
    tap_slice = lax.dynamic_slice_in_dim(conv_taps, shard_index * channels, channels, 1)
    mixed_conv = (
        padded[:-2] * tap_slice[0] + padded[1:-1] * tap_slice[1] + padded[2:] * tap_slice[2]
    )
    conv_mixed = (mixed_conv * jax.nn.silu(rounded(gate_pre))).astype(jnp.bfloat16)
    queries = (probe_before_norm * (1.0 / math.sqrt(KEY_DIM))).astype(jnp.bfloat16)
    key_rows = key_pre.astype(jnp.bfloat16)
    values = value_pre.astype(jnp.bfloat16)
    low_rank = project(normed, decay_down).astype(jnp.bfloat16)
    key_offset = shard_index * key_width
    up_slice = lax.dynamic_slice_in_dim(decay_up, key_offset, key_width, 1)
    bias_slice = lax.dynamic_slice_in_dim(decay_bias, key_offset, key_width, 0)
    log_decay = jax.nn.log_sigmoid(project(low_rank, up_slice) + bias_slice) / 16.0
    log_decay = log_decay.reshape(length, head_count, KEY_DIM) + decay_extra.T[:, :, None]
    raw_mixed = gla_heads(
        queries.reshape(length, head_count, KEY_DIM),
        key_rows.reshape(length, head_count, KEY_DIM),
        values.reshape(length, head_count, VAL_DIM),
        log_decay,
    )
    gain_slice = lax.dynamic_slice_in_dim(head_gain, shard_index * val_width, val_width, 0).reshape(
        head_count, VAL_DIM
    )
    gla_mixed = rms_rows(raw_mixed, gain_slice).astype(jnp.bfloat16).reshape(length, val_width)
    mixed = sum_at_owner(
        (project(conv_mixed, conv_out_full) + project(gla_mixed, value_out_full)).astype(
            jnp.bfloat16
        ),
        "tp",
        0,
    )
    return mixed.astype(jnp.bfloat16)


def solution(mesh):
    torus = Mesh(mesh.devices.reshape(16, 4, mesh.shape["tp"]), ("sp_0", "sp_1", "tp"))
    return jax.shard_map(
        local,
        mesh=torus,
        in_specs=(
            P(SP_TP, None),
            P(),
            P(SP, "tp"),
            P(SP, "tp"),
            P(),
            P(SP, "tp"),
            P(SP, "tp"),
            P(SP, "tp"),
            P(),
            P(),
            P(),
            P("tp", SP),
            P(),
            P("tp", SP),
            P("tp", SP),
        ),
        out_specs=P(SP_TP, None),
        check_vma=False,
    )
```

profile of v0, /device:TPU:1, one launch (start us, length us, event | category | flops | bytes accessed | tf_op | source)
XLA Modules:
  0.0 377.7 jit_solution(13934947043964088281)
XLA Ops:
  6.5 0.8 constant_dynamic-update-slice_fusion.6
  7.3 0.7 constant_dynamic-update-slice_fusion.5
  8.0 0.7 constant_dynamic-update-slice_fusion.4
  8.7 0.7 constant_dynamic-update-slice_fusion.3
  9.4 0.7 constant_dynamic-update-slice_fusion.2
  10.1 0.7 constant_dynamic-update-slice_fusion.1
  10.9 0.7 constant_dynamic-update-slice_fusion
  12.3 2.3 broadcast_in_dim.36
  14.5 10.5 %all-to-all-start = ((bf16[8,48,2048]{2,1,0:T(8,128)(2,1)}), bf16[8,48,2048]{2,1,0:T(8,128)(2,1)S(1)}, u32[]{:S(2)}, u32[]{:S(2)}) async-start(bf16[8,48,2048]{2,1,0:T(8,128)(2,1)} %broadcast_in_dim.36), calls=%async_computation | async-start | bytes 3145728 | tf_op jit(solution)/shard_map/all_to_all | solution.py:45
  25.0 0.8 dynamic_slice.14
  25.8 19.8 %all-to-all-done = bf16[8,48,2048]{2,1,0:T(8,128)(2,1)S(1)} async-done(((bf16[8,48,2048]{2,1,0:T(8,128)(2,1)}), bf16[8,48,2048]{2,1,0:T(8,128)(2,1)S(1)}, u32[]{:S(2)}, u32[]{:S(2)}) %all-to-all-start) | async-done | bytes 1572896 | tf_op jit(solution)/shard_map/all_to_all | solution.py:45
  46.5 1.5 fusion.58
  48.6 5.9 %all-gather.3 = bf16[4,1,128]{2,1,0:T(2,128)(2,1)S(1)} all-gather(bf16[1,1,128]{2,1,0:T(2,128)(2,1)S(1)} %convert_bitcast_fusion), channel_id=2, replica_groups=mesh['sp_0'=16,'sp_1'=4,'tp'=8] {'sp_1'}, dimensions={0}, use_global_device_ids=true | all-gather | bytes 1280 | tf_op jit(solution)/shard_map/all_gather | solution.py:28
  55.1 105.2 %all-gather.8.cloned.1.call-done = bf16[2048,1536]{1,0:T(8,128)(2,1)} async-done(((bf16[32,1536]{1,0:T(8,128)(2,1)}), bf16[2048,1536]{1,0:T(8,128)(2,1)}) %all-gather.8.cloned.1.call-update) | async-done | bytes 6291472 | tf_op jit(solution)/shard_map/all_gather | solution.py:65
  160.4 1.6 convolution_convert_fusion.3
  162.0 1.8 convolution_convert_fusion
  164.5 9.4 %all-gather.2 = bf16[512,256]{1,0:T(8,128)(2,1)S(1)} all-gather(bf16[128,256]{1,0:T(8,128)(2,1)S(1)} %bitcast.364), channel_id=4, replica_groups=mesh['sp_0'=16,'sp_1'=4,'tp'=8] {'sp_1'}, dimensions={0}, use_global_device_ids=true | all-gather | bytes 327680 | tf_op jit(solution)/shard_map/all_gather | solution.py:28
  174.6 10.3 %all-gather.1 = bf16[512,256]{1,0:T(8,128)(2,1)S(1)} all-gather(bf16[128,256]{1,0:T(8,128)(2,1)S(1)} %bitcast.365), channel_id=3, replica_groups=mesh['sp_0'=16,'sp_1'=4,'tp'=8] {'sp_1'}, dimensions={0}, use_global_device_ids=true | all-gather | bytes 327680 | tf_op jit(solution)/shard_map/all_gather | solution.py:28
  184.9 0.8 fusion.87
  185.9 1.3 dynamic_slice.15
  188.3 0.9 constant_dynamic-slice_fusion
  189.2 0.7 copy.40
  189.9 0.7 copy.56
  190.7 0.7 copy.47
  191.4 0.7 copy.43
  192.1 0.7 copy.53
  192.9 20.4 %all_gather.43 = bf16[16,1,128]{2,1,0:T(2,128)(2,1)S(1)} all-gather(bf16[1,1,128]{2,1,0:T(2,128)(2,1)S(1)} %get-tuple-element.51), channel_id=1, replica_groups=mesh['sp_0'=16,'sp_1'=4,'tp'=8] {'sp_0'}, dimensions={0}, use_global_device_ids=true | all-gather | bytes 4352 | tf_op jit(solution)/shard_map/all_gather | solution.py:28
  213.3 19.5 %all_gather.39 = bf16[16,1,128]{2,1,0:T(2,128)(2,1)S(1)} all-gather(bf16[1,1,128]{2,1,0:T(2,128)(2,1)S(1)} %get-tuple-element.52), channel_id=1, replica_groups=mesh['sp_0'=16,'sp_1'=4,'tp'=8] {'sp_0'}, dimensions={0}, use_global_device_ids=true | all-gather | bytes 4352 | tf_op jit(solution)/shard_map/all_gather | solution.py:28
  235.1 1.8 convolution_convert_fusion.2
  236.9 1.9 collective-permute-start
  238.8 1.3 collective-permute-start.1
  240.1 1.6 fusion.8
  241.8 1.8 convolution_convert_fusion.1
  243.6 0.9 convolution_select_fusion.1
  244.5 1.9 fusion.17
  246.5 7.6 %all-gather.10.cloned.1.call-done = bf16[16,1,128,256]{3,2,1,0:T(8,128)(2,1)} async-done(((bf16[1,1,128,256]{3,2,1,0:T(8,128)(2,1)}), bf16[16,1,128,256]{3,2,1,0:T(8,128)(2,1)}) %all-gather.10.cloned.1.call-update) | async-done | bytes 1048592 | tf_op jit(solution)/shard_map/all_gather | solution.py:28
  254.1 2.0 fusion.86
  256.2 1.6 fusion.3
  257.8 1.0 fusion.22
  258.8 65.4 %all-gather.12.cloned.1.call-done = bf16[16,1,128,256]{3,2,1,0:T(8,128)(2,1)} async-done(((bf16[1,1,128,256]{3,2,1,0:T(8,128)(2,1)}), bf16[16,1,128,256]{3,2,1,0:T(8,128)(2,1)}) %all-gather.12.cloned.1.call-update) | async-done | bytes 1048592 | tf_op jit(solution)/shard_map/all_gather | solution.py:28
  324.2 2.0 fusion.79
  326.3 1.7 fusion.5
  328.1 1.0 convolution_add_fusion.1
  329.0 2.5 fusion.42
  331.6 1.1 fusion.41
  332.7 1.8 add_convert_fusion
  334.6 35.6 %all_to_all.10 = bf16[8,48,2048]{2,1,0:T(8,128)(2,1)S(1)} all-to-all(bf16[8,48,2048]{2,1,0:T(8,128)(2,1)S(1)} %bitcast.348), channel_id=1, replica_groups=mesh['sp_0'=16,'sp_1'=4,'tp'=8] {'tp'}, dimensions={0} | all-to-all | bytes 3145728 | tf_op jit(solution)/shard_map/all_to_all | solution.py:95
  370.2 0.9 reduce_sum.42
  (85 shorter events, 7.8 us)
Async XLA Ops:
  6.5 40.0 %copy-start = (bf16[2048,16]{0,1:T(8,128)(2,1)S(1)}, bf16[2048,16]{0,1:T(8,128)(2,1)}, u32[]{:S(2)}) copy-start(bf16[2048,16]{0,1:T(8,128)(2,1)} %param.23) | copy-start | bytes 196612
  6.5 153.8 %all-gather.8.cloned.1.call-start = ((), (), s32[]{:S(2)}) async-start(), calls=%async_computation.2 | async-start | bytes 6389760 | tf_op jit(solution)/shard_map/all_gather | solution.py:65
  11.6 0.7 copy-start.12
  14.5 11.2 %copy-start.20 = (f32[1,384]{1,0:T(1,128)S(1)}, f32[1,384]{1,0:T(1,128)}, u32[]{:S(2)}) copy-start(f32[1,384]{1,0:T(1,128)} %param.26) | copy-start | bytes 4612
  14.5 31.1 %all-to-all-start = ((bf16[8,48,2048]{2,1,0:T(8,128)(2,1)}), bf16[8,48,2048]{2,1,0:T(8,128)(2,1)S(1)}, u32[]{:S(2)}, u32[]{:S(2)}) async-start(bf16[8,48,2048]{2,1,0:T(8,128)(2,1)} %broadcast_in_dim.36), calls=%async_computation | async-start | bytes 3145728 | tf_op jit(solution)/shard_map/all_to_all | solution.py:45
  25.0 21.1 %copy-start.13 = (f32[2048]{0:T(1024)S(1)}, f32[2048]{0:T(1024)}, u32[]{:S(2)}) copy-start(f32[2048]{0:T(1024)} %param.16) | copy-start | bytes 24580
  25.0 229.1 %all-gather.10.cloned.1.call-start = ((), (), s32[]{:S(2)}) async-start(), calls=%async_computation.3 | async-start | bytes 1114112 | tf_op jit(solution)/shard_map/all_gather | solution.py:28
  48.1 115.7 %copy-start.1 = (f32[384,128]{1,0:T(8,128)}, f32[384,128]{1,0:T(8,128)S(1)}, u32[]{:S(2)}) copy-start(f32[384,128]{1,0:T(8,128)S(1)} %fusion.58) | copy-start | bytes 589828
  163.8 10.4 %copy-start.5 = (bf16[384,256]{1,0:T(8,128)(2,1)}, bf16[384,256]{1,0:T(8,128)(2,1)S(1)}, u32[]{:S(2)}) copy-start(bf16[384,256]{1,0:T(8,128)(2,1)S(1)} %convolution_convert_fusion) | copy-start | bytes 589828
  164.1 10.5 %copy-start.11 = (bf16[6,128,256]{2,1,0:T(8,128)(2,1)}, bf16[6,128,256]{2,1,0:T(8,128)(2,1)S(1)}, u32[]{:S(2)}) copy-start(bf16[6,128,256]{2,1,0:T(8,128)(2,1)S(1)} %fusion.89) | copy-start | bytes 1179652
  173.9 11.0 %copy-start.3 = (bf16[512,256]{1,0:T(8,128)(2,1)}, bf16[512,256]{1,0:T(8,128)(2,1)S(1)}, u32[]{:S(2)}) copy-start(bf16[512,256]{1,0:T(8,128)(2,1)S(1)} %all-gather.2) | copy-start | bytes 786436
  174.2 11.6 %copy-start.10 = (bf16[6,128,256]{2,1,0:T(8,128)(2,1)}, bf16[6,128,256]{2,1,0:T(8,128)(2,1)S(1)}, u32[]{:S(2)}) copy-start(bf16[6,128,256]{2,1,0:T(8,128)(2,1)S(1)} %fusion.54) | copy-start | bytes 1179652
  184.9 0.9 copy-start.4
  185.8 138.4 %all-gather.12.cloned.1.call-start = ((), (), s32[]{:S(2)}) async-start(), calls=%async_computation.4 | async-start | bytes 1114112 | tf_op jit(solution)/shard_map/all_gather | solution.py:28
  236.9 7.5 %collective-permute-start = (bf16[1,256]{1,0:T(2,128)(2,1)S(1)}, bf16[1,256]{1,0:T(2,128)(2,1)S(1)}, u32[]{:S(2)}, u32[]{:S(2)}) collective-permute-start(bf16[1,256]{1,0:T(2,128)(2,1)S(1)} %get-tuple-element.10), channel_id=1, source_target_pairs={{0,8},{8,16},{16,24},{24,32},{32,40},{40,48},{48,56},{56,64},{64,7... | collective-permute-start | bytes 1544 | tf_op jit(solution)/shard_map/ppermute | solution.py:80
  238.8 5.7 %collective-permute-start.1 = (bf16[1,256]{1,0:T(2,128)(2,1)S(1)}, bf16[1,256]{1,0:T(2,128)(2,1)S(1)}, u32[]{:S(2)}, u32[]{:S(2)}) collective-permute-start(bf16[1,256]{1,0:T(2,128)(2,1)S(1)} %get-tuple-element.11), channel_id=1, source_target_pairs={{8,0},{16,8},{24,16},{32,24},{40,32},{48,40},{56,48},{64,56},{72,6... | collective-permute-start | bytes 1544 | tf_op jit(solution)/shard_map/ppermute | solution.py:83
  241.7 1.9 copy-start.6
  254.1 3.7 copy-start.7
  256.1 68.1 %copy-start.15 = (f32[128]{0:T(128)S(1)}, f32[128]{0:T(128)}, u32[]{:S(2)}) copy-start(f32[128]{0:T(128)} %get-tuple-element.47) | copy-start | bytes 1540
  256.1 68.1 %copy-start.16 = (f32[128]{0:T(128)S(1)}, f32[128]{0:T(128)}, u32[]{:S(2)}) copy-start(f32[128]{0:T(128)} %get-tuple-element.15) | copy-start | bytes 1540
  256.1 68.1 %copy-start.17 = (f32[128]{0:T(128)S(1)}, f32[128]{0:T(128)}, u32[]{:S(2)}) copy-start(f32[128]{0:T(128)} %get-tuple-element.16) | copy-start | bytes 1540
  256.1 68.1 %copy-start.18 = (f32[128]{0:T(128)S(1)}, f32[128]{0:T(128)}, u32[]{:S(2)}) copy-start(f32[128]{0:T(128)} %get-tuple-element.17) | copy-start | bytes 1540
  256.2 68.1 %copy-start.19 = (f32[128]{0:T(128)S(1)}, f32[128]{0:T(128)}, u32[]{:S(2)}) copy-start(f32[128]{0:T(128)} %get-tuple-element.18) | copy-start | bytes 1540
  326.3 1.8 copy-start.2
  326.3 1.8 copy-start.8
  326.3 1.8 copy-start.9
  328.0 3.6 copy-start.14
Sparse Core Ops, SparseCore 0:
  12.4 147.9 all-gather.7
  185.9 68.0 all-gather.9
  256.2 67.9 all-gather.11
where the time goes:
time: 379 us; the launch traced here: 378 us
  waiting for transfers between devices  198 us (52%)
  blocking collectives  101 us (27%)
  matrix products  24 us (6%)
  local copies, waits for them, and re-layouts  15.1 us (4%)
  starting transfers between devices  13.7 us (4%)
  between operations  13.6 us (4%)
  other arithmetic  12.1 us (3%)
    all_gather x1, waiting for transfers between devices, rows_first(): filled = lax.all_gather(both, axis, axis=0, tiled=True)  105 us
    all_gather x2, waiting for transfers between devices, prefix_by_axis(): lax.all_gather(part.astype(kind), axis)  73 us
    all_gather x5, blocking collectives, prefix_by_axis(): lax.all_gather(part.astype(kind), axis)  65.4 us
    all_to_all x1, blocking collectives, sum_at_owner(): lax.all_to_all(blocks, axis, split_axis=0, concat_axis=0, tiled=True)  35.6 us
    all_to_all x1, waiting for transfers between devices, copy_for_each(): lax.all_to_all(jnp.broadcast_to(array[None], (count, *array.shape)), axis...  19.8 us
    dot_general x8, matrix products, project(): return jnp.dot(normed, weight, preferred_element_type=jnp.float32)  14 us
    all_to_all x1, starting transfers between devices, copy_for_each(): lax.all_to_all(jnp.broadcast_to(array[None], (count, *array.shape)), axis...  10.5 us
  transfers between devices with their start and end apart: 6, of which 4 were waited for; matrix products, arithmetic and copies ran while one was open for 8% of the time, Pallas kernels for 0%

commit v1 on v0

--- a/solution.py
+++ b/solution.py
@@ -62,7 +62,9 @@
     turned = [jnp.moveaxis(a, dim, 0) for a, dim in zip(arrays, dims)]
     widths = [t[0].size for t in turned]
     both = jnp.concatenate([t.reshape(-1, w) for t, w in zip(turned, widths)], axis=1)
-    filled = lax.all_gather(both, axis, axis=0, tiled=True)
+    filled = jnp.concatenate(
+        lax.all_to_all(jnp.stack([both] * lax.axis_size(axis)), axis, 0, 0), axis=0
+    )
     blocks = jnp.split(filled, [sum(widths[:k]) for k in range(1, len(widths))], axis=1)
     return tuple(
         (

time: 379 us -> 543 us (1.43)
  waiting for transfers between devices: 198 us -> 340 us
  starting transfers between devices: 13.7 us -> 30.1 us
  blocking collectives: 101 us -> 109 us
    all_to_all x0 -> x1, waiting for transfers between devices: none -> 259 us  [rows_first(): lax.all_to_all(jnp.stack([both] * lax.axis_size(axis)), axis, 0, 0)]
    all_gather x1 -> x0, waiting for transfers between devices: 105 us -> none  [rows_first(): filled = lax.all_gather(both, axis, axis=0, tiled=True)]
    all_to_all x0 -> x1, starting transfers between devices: none -> 14.3 us  [rows_first(): lax.all_to_all(jnp.stack([both] * lax.axis_size(axis)), axis, 0, 0)]
    all_gather x2, waiting for transfers between devices: 73 us -> 60.1 us  [prefix_by_axis(): lax.all_gather(part.astype(kind), axis)]
    all_gather x5, blocking collectives: 65.4 us -> 72.9 us  [prefix_by_axis(): lax.all_gather(part.astype(kind), axis)]
  transfers between devices with their start and end apart: 6 -> 6, of which waited for: 4 -> 3; matrix products, arithmetic and copies ran while one was open for 8% -> 5% of each run, Pallas kernels for 0% -> 0%
where the time goes in v1:
time: 543 us; the launch traced here: 542 us
  waiting for transfers between devices  340 us (63%)
  blocking collectives  109 us (20%)
  starting transfers between devices  30.1 us (6%)
  matrix products  24 us (4%)
  between operations  14.1 us (3%)
  local copies, waits for them, and re-layouts  13 us (2%)
  other arithmetic  12.3 us (2%)
    all_to_all x1, waiting for transfers between devices, rows_first(): lax.all_to_all(jnp.stack([both] * lax.axis_size(axis)), axis, 0, 0)  259 us
    all_gather x5, blocking collectives, prefix_by_axis(): lax.all_gather(part.astype(kind), axis)  72.9 us
    all_gather x2, waiting for transfers between devices, prefix_by_axis(): lax.all_gather(part.astype(kind), axis)  60.1 us
    all_to_all x1, blocking collectives, sum_at_owner(): lax.all_to_all(blocks, axis, split_axis=0, concat_axis=0, tiled=True)  35.7 us
    all_to_all x1, waiting for transfers between devices, copy_for_each(): lax.all_to_all(jnp.broadcast_to(array[None], (count, *array.shape)), axis...  20.5 us
    all_to_all x1, starting transfers between devices, rows_first(): lax.all_to_all(jnp.stack([both] * lax.axis_size(axis)), axis, 0, 0)  14.3 us
    dot_general x8, matrix products, project(): return jnp.dot(normed, weight, preferred_element_type=jnp.float32)  14 us
  transfers between devices with their start and end apart: 6, of which 3 were waited for; matrix products, arithmetic and copies ran while one was open for 5% of the time, Pallas kernels for 0%

profile of v1, /device:TPU:1, one launch (start us, length us, event | category | flops | bytes accessed | tf_op | source)
XLA Modules:
  0.0 541.6 jit_solution(2652016022174196841)
XLA Ops:
  6.6 2.4 broadcast_in_dim.36
  9.0 10.3 %all-to-all-start = ((bf16[8,48,2048]{2,1,0:T(8,128)(2,1)}), bf16[8,48,2048]{2,1,0:T(8,128)(2,1)S(1)}, u32[]{:S(2)}, u32[]{:S(2)}) async-start(bf16[8,48,2048]{2,1,0:T(8,128)(2,1)} %broadcast_in_dim.36), calls=%async_computation | async-start | bytes 3145728 | tf_op jit(solution)/shard_map/all_to_all | solution.py:45
  19.4 20.5 %all-to-all-done = bf16[8,48,2048]{2,1,0:T(8,128)(2,1)S(1)} async-done(((bf16[8,48,2048]{2,1,0:T(8,128)(2,1)}), bf16[8,48,2048]{2,1,0:T(8,128)(2,1)S(1)}, u32[]{:S(2)}, u32[]{:S(2)}) %all-to-all-start) | async-done | bytes 1572896 | tf_op jit(solution)/shard_map/all_to_all | solution.py:45
  39.9 3.4 stack.2
  43.3 14.3 %all-to-all-start.1 = ((bf16[64,32,1536]{2,1,0:T(8,128)(2,1)}), bf16[64,32,1536]{2,1,0:T(8,128)(2,1)}, u32[]{:S(2)}, u32[]{:S(2)}) async-start(bf16[64,32,1536]{2,1,0:T(8,128)(2,1)} %stack.2), calls=%async_computation.1 | async-start | bytes 12582912 | tf_op jit(solution)/shard_map/all_to_all | solution.py:66
  57.7 0.8 dynamic_slice.14
  58.5 1.3 dynamic_slice.15
  60.7 1.5 fusion.58
  62.8 8.2 %all-gather.3 = bf16[4,1,128]{2,1,0:T(2,128)(2,1)S(1)} all-gather(bf16[1,1,128]{2,1,0:T(2,128)(2,1)S(1)} %convert_bitcast_fusion), channel_id=2, replica_groups=mesh['sp_0'=16,'sp_1'=4,'tp'=8] {'sp_1'}, dimensions={0}, use_global_device_ids=true | all-gather | bytes 1280 | tf_op jit(solution)/shard_map/all_gather | solution.py:28
  71.0 0.6 broadcast_select_fusion.3
  71.6 258.9 %all-to-all-done.1 = bf16[64,32,1536]{2,1,0:T(8,128)(2,1)} async-done(((bf16[64,32,1536]{2,1,0:T(8,128)(2,1)}), bf16[64,32,1536]{2,1,0:T(8,128)(2,1)}, u32[]{:S(2)}, u32[]{:S(2)}) %all-to-all-start.1) | async-done | bytes 6291488 | tf_op jit(solution)/shard_map/all_to_all | solution.py:66
  330.5 1.8 convolution_convert_fusion
  332.3 1.7 convolution_convert_fusion.3
  335.1 9.4 %all-gather.2 = bf16[512,256]{1,0:T(8,128)(2,1)S(1)} all-gather(bf16[128,256]{1,0:T(8,128)(2,1)S(1)} %bitcast.365), channel_id=4, replica_groups=mesh['sp_0'=16,'sp_1'=4,'tp'=8] {'sp_1'}, dimensions={0}, use_global_device_ids=true | all-gather | bytes 327680 | tf_op jit(solution)/shard_map/all_gather | solution.py:28
  344.8 10.1 %all-gather.1 = bf16[512,256]{1,0:T(8,128)(2,1)S(1)} all-gather(bf16[128,256]{1,0:T(8,128)(2,1)S(1)} %bitcast.366), channel_id=3, replica_groups=mesh['sp_0'=16,'sp_1'=4,'tp'=8] {'sp_1'}, dimensions={0}, use_global_device_ids=true | all-gather | bytes 327680 | tf_op jit(solution)/shard_map/all_gather | solution.py:28
  355.0 0.8 fusion.87
  355.9 0.6 iota_compare_fusion.3
  356.5 0.6 iota_compare_fusion.2
  357.1 0.9 constant_dynamic-slice_fusion
  358.0 0.7 copy.56
  358.7 0.7 copy.40
  359.4 0.7 copy.47
  360.2 0.7 copy.43
  360.9 0.7 copy.53
  361.6 25.3 %all_gather.35 = bf16[16,1,128]{2,1,0:T(2,128)(2,1)S(1)} all-gather(bf16[1,1,128]{2,1,0:T(2,128)(2,1)S(1)} %get-tuple-element.52), channel_id=1, replica_groups=mesh['sp_0'=16,'sp_1'=4,'tp'=8] {'sp_0'}, dimensions={0}, use_global_device_ids=true | all-gather | bytes 4352 | tf_op jit(solution)/shard_map/all_gather | solution.py:28
  386.9 19.9 %all_gather.39 = bf16[16,1,128]{2,1,0:T(2,128)(2,1)S(1)} all-gather(bf16[1,1,128]{2,1,0:T(2,128)(2,1)S(1)} %get-tuple-element.51), channel_id=1, replica_groups=mesh['sp_0'=16,'sp_1'=4,'tp'=8] {'sp_0'}, dimensions={0}, use_global_device_ids=true | all-gather | bytes 4352 | tf_op jit(solution)/shard_map/all_gather | solution.py:28
  406.8 0.6 fusion.115
  407.9 0.7 fusion.130
  408.6 0.7 fusion.113
  409.2 1.8 convolution_convert_fusion.2
  411.1 1.3 collective-permute-start.1
  412.4 4.2 collective-permute-start
  416.5 1.6 fusion.8
  418.2 1.8 convolution_convert_fusion.1
  420.0 0.9 convolution_select_fusion.1
  420.9 1.9 fusion.17
  423.0 2.1 fusion.86
  425.0 1.6 fusion.3
  426.7 1.0 fusion.22
  427.6 60.1 %all-gather.9.cloned.1.call-done = bf16[16,1,128,256]{3,2,1,0:T(8,128)(2,1)} async-done(((bf16[1,1,128,256]{3,2,1,0:T(8,128)(2,1)}), bf16[16,1,128,256]{3,2,1,0:T(8,128)(2,1)}) %all-gather.9.cloned.1.call-update) | async-done | bytes 1048592 | tf_op jit(solution)/shard_map/all_gather | solution.py:28
  487.7 2.1 fusion.79
  489.9 1.7 fusion.5
  491.6 1.0 convolution_add_fusion.1
  492.6 2.5 fusion.42
  495.1 1.1 fusion.41
  496.2 1.8 add_convert_fusion
  498.1 35.7 %all_to_all.15 = bf16[8,48,2048]{2,1,0:T(8,128)(2,1)S(1)} all-to-all(bf16[8,48,2048]{2,1,0:T(8,128)(2,1)S(1)} %bitcast.349), channel_id=1, replica_groups=mesh['sp_0'=16,'sp_1'=4,'tp'=8] {'tp'}, dimensions={0} | all-to-all | bytes 3145728 | tf_op jit(solution)/shard_map/all_to_all | solution.py:97
  533.8 0.9 reduce_sum.42
  (95 shorter events, 3.8 us)
Async XLA Ops:
  6.5 54.2 %copy-start = (bf16[2048,16]{0,1:T(8,128)(2,1)S(1)}, bf16[2048,16]{0,1:T(8,128)(2,1)}, u32[]{:S(2)}) copy-start(bf16[2048,16]{0,1:T(8,128)(2,1)} %param.23) | copy-start | bytes 196612
  6.5 12.8 %copy-start.12 = (bf16[32,256]{1,0:T(8,128)(2,1)S(1)}, bf16[32,256]{1,0:T(8,128)(2,1)}, u32[]{:S(2)}) copy-start(bf16[32,256]{1,0:T(8,128)(2,1)} %param.17) | copy-start | bytes 49156
  6.5 12.8 %copy-start.13 = (bf16[32,256]{1,0:T(8,128)(2,1)S(1)}, bf16[32,256]{1,0:T(8,128)(2,1)}, u32[]{:S(2)}) copy-start(bf16[32,256]{1,0:T(8,128)(2,1)} %param.18) | copy-start | bytes 49156
  6.5 12.8 %copy-start.18 = (bf16[32,128]{1,0:T(8,128)(2,1)S(1)}, bf16[32,128]{1,0:T(8,128)(2,1)}, u32[]{:S(2)}) copy-start(bf16[32,128]{1,0:T(8,128)(2,1)} %param.20) | copy-start | bytes 24580
  6.5 12.8 %copy-start.19 = (bf16[32,128]{1,0:T(8,128)(2,1)S(1)}, bf16[32,128]{1,0:T(8,128)(2,1)}, u32[]{:S(2)}) copy-start(bf16[32,128]{1,0:T(8,128)(2,1)} %param.21) | copy-start | bytes 24580
  6.5 12.8 %copy-start.14 = (bf16[32,256]{1,0:T(8,128)(2,1)S(1)}, bf16[32,256]{1,0:T(8,128)(2,1)}, u32[]{:S(2)}) copy-start(bf16[32,256]{1,0:T(8,128)(2,1)} %param.22) | copy-start | bytes 49156
  6.6 12.8 %copy-start.15 = (bf16[256,32]{0,1:T(8,128)(2,1)S(1)}, bf16[256,32]{0,1:T(8,128)(2,1)}, u32[]{:S(2)}) copy-start(bf16[256,32]{0,1:T(8,128)(2,1)} %param.28) | copy-start | bytes 49156
  6.6 12.8 %copy-start.16 = (bf16[256,32]{0,1:T(8,128)(2,1)S(1)}, bf16[256,32]{0,1:T(8,128)(2,1)}, u32[]{:S(2)}) copy-start(bf16[256,32]{0,1:T(8,128)(2,1)} %param.29) | copy-start | bytes 49156
  9.0 30.9 %all-to-all-start = ((bf16[8,48,2048]{2,1,0:T(8,128)(2,1)}), bf16[8,48,2048]{2,1,0:T(8,128)(2,1)S(1)}, u32[]{:S(2)}, u32[]{:S(2)}) async-start(bf16[8,48,2048]{2,1,0:T(8,128)(2,1)} %broadcast_in_dim.36), calls=%async_computation | async-start | bytes 3145728 | tf_op jit(solution)/shard_map/all_to_all | solution.py:45
  43.3 14.4 %copy-start.24 = (f32[1,384]{1,0:T(1,128)S(1)}, f32[1,384]{1,0:T(1,128)}, u32[]{:S(2)}) copy-start(f32[1,384]{1,0:T(1,128)} %param.26) | copy-start | bytes 4612
  43.3 17.0 %copy-start.17 = (f32[2048]{0:T(1024)S(1)}, f32[2048]{0:T(1024)}, u32[]{:S(2)}) copy-start(f32[2048]{0:T(1024)} %param.16) | copy-start | bytes 24580
  43.3 287.2 %all-to-all-start.1 = ((bf16[64,32,1536]{2,1,0:T(8,128)(2,1)}), bf16[64,32,1536]{2,1,0:T(8,128)(2,1)}, u32[]{:S(2)}, u32[]{:S(2)}) async-start(bf16[64,32,1536]{2,1,0:T(8,128)(2,1)} %stack.2), calls=%async_computation.1 | async-start | bytes 12582912 | tf_op jit(solution)/shard_map/all_to_all | solution.py:66
  57.5 365.4 %all-gather.7.cloned.1.call-start = ((), (), s32[]{:S(2)}) async-start(), calls=%async_computation.3 | async-start | bytes 1114112 | tf_op jit(solution)/shard_map/all_gather | solution.py:28
  62.3 272.1 %copy-start.1 = (f32[384,128]{1,0:T(8,128)}, f32[384,128]{1,0:T(8,128)S(1)}, u32[]{:S(2)}) copy-start(f32[384,128]{1,0:T(8,128)S(1)} %fusion.58) | copy-start | bytes 589828
  332.3 2.8 copy-start.5
  334.3 76.7 %copy-start.10 = (bf16[6,128,256]{2,1,0:T(8,128)(2,1)}, bf16[6,128,256]{2,1,0:T(8,128)(2,1)S(1)}, u32[]{:S(2)}) copy-start(bf16[6,128,256]{2,1,0:T(8,128)(2,1)S(1)} %fusion.54) | copy-start | bytes 1179652
  334.7 76.4 %copy-start.11 = (bf16[6,128,256]{2,1,0:T(8,128)(2,1)}, bf16[6,128,256]{2,1,0:T(8,128)(2,1)S(1)}, u32[]{:S(2)}) copy-start(bf16[6,128,256]{2,1,0:T(8,128)(2,1)S(1)} %fusion.89) | copy-start | bytes 1179652
  344.5 10.5 %copy-start.3 = (bf16[512,256]{1,0:T(8,128)(2,1)}, bf16[512,256]{1,0:T(8,128)(2,1)S(1)}, u32[]{:S(2)}) copy-start(bf16[512,256]{1,0:T(8,128)(2,1)S(1)} %all-gather.2) | copy-start | bytes 786436
  355.0 0.8 copy-start.4
  355.9 131.8 %all-gather.9.cloned.1.call-start = ((), (), s32[]{:S(2)}) async-start(), calls=%async_computation.4 | async-start | bytes 1114112 | tf_op jit(solution)/shard_map/all_gather | solution.py:28
  411.1 9.8 %collective-permute-start.1 = (bf16[1,256]{1,0:T(2,128)(2,1)S(1)}, bf16[1,256]{1,0:T(2,128)(2,1)S(1)}, u32[]{:S(2)}, u32[]{:S(2)}) collective-permute-start(bf16[1,256]{1,0:T(2,128)(2,1)S(1)} %get-tuple-element.11), channel_id=1, source_target_pairs={{8,0},{16,8},{24,16},{32,24},{40,32},{48,40},{56,48},{64,56},{72,6... | collective-permute-start | bytes 1544 | tf_op jit(solution)/shard_map/ppermute | solution.py:85
  412.4 8.5 %collective-permute-start = (bf16[1,256]{1,0:T(2,128)(2,1)S(1)}, bf16[1,256]{1,0:T(2,128)(2,1)S(1)}, u32[]{:S(2)}, u32[]{:S(2)}) collective-permute-start(bf16[1,256]{1,0:T(2,128)(2,1)S(1)} %get-tuple-element.10), channel_id=1, source_target_pairs={{0,8},{8,16},{16,24},{24,32},{32,40},{40,48},{48,56},{56,64},{64,7... | collective-permute-start | bytes 1544 | tf_op jit(solution)/shard_map/ppermute | solution.py:82
  418.2 2.8 copy-start.6
  422.9 64.8 %copy-start.21 = (f32[128]{0:T(128)S(1)}, f32[128]{0:T(128)}, u32[]{:S(2)}) copy-start(f32[128]{0:T(128)} %get-tuple-element.47) | copy-start | bytes 1540
  422.9 64.8 %copy-start.22 = (f32[128]{0:T(128)S(1)}, f32[128]{0:T(128)}, u32[]{:S(2)}) copy-start(f32[128]{0:T(128)} %get-tuple-element.15) | copy-start | bytes 1540
  422.9 64.8 %copy-start.23 = (f32[128]{0:T(128)S(1)}, f32[128]{0:T(128)}, u32[]{:S(2)}) copy-start(f32[128]{0:T(128)} %get-tuple-element.16) | copy-start | bytes 1540
  422.9 3.7 copy-start.7
  425.0 64.9 %copy-start.25 = (pred[6,6]{1,0:T(8,128)(4,1)S(1)}, pred[6,6]{1,0:T(8,128)(4,1)}, u32[]{:S(2)}) copy-start(pred[6,6]{1,0:T(8,128)(4,1)} %iota_compare_fusion.2) | copy-start | bytes 112
  487.7 3.9 copy-start.2
  487.7 3.9 copy-start.8
  487.7 3.9 copy-start.9
  489.9 5.2 copy-start.20
Sparse Core Ops, SparseCore 0:
  356.0 61.7 all-gather.6
  419.9 67.7 all-gather.8
